TPU v7x, 32 devices: a whole 2x2x4 slice. The times are simulated.
32 devices in a mesh: ep: 4 (over y, x), tp: 8 (over z, core).
Axes of the slice: x: 2, y: 2, z: 4, core: 2. Of those that a mesh axis runs over, the one named last changes fastest.
Arguments:
- tokens: bfloat16 [1024, 4096], P('ep'), may hold values from -6 to 6
- cotangent: bfloat16 [1024, 4096], P('ep'), may hold values from -6 to 6
- routing: int32 [1024, 2], P('ep'), may hold values from 0 to 3, all different within a row; in each aligned block of 256 rows (0 to 255, 256 to 511, ...) at most 160 rows name the same one
- group_gate: float32 [1024], P('ep'), may hold values from 0.2 to 1
- inner_gate: float32 [1024, 2], P('ep'), may hold values from 0.1 to 0.9
- w_gate: bfloat16 [4, 4096, 2048], P('ep', None, 'tp'), may hold values from -0.09375 to 0.09375
- w_up: bfloat16 [4, 4096, 2048], P('ep', None, 'tp'), may hold values from -0.09375 to 0.09375
- w_down: bfloat16 [4, 2048, 4096], P('ep', 'tp'), may hold values from -0.125 to 0.125
Outputs:
- token_grad: bfloat16 [1024, 4096], P('ep', 'tp')
- group_grad: float32 [1024], P('ep')
- inner_grad: float32 [1024, 2], P('ep')
- gate_weight_grad: bfloat16 [4, 4096, 2048], P('ep', None, 'tp')
- up_weight_grad: bfloat16 [4, 4096, 2048], P('ep', None, 'tp')
- down_weight_grad: bfloat16 [4, 2048, 4096], P('ep', 'tp')
Inputs may be any that keep to these rules, and one draw needn't show every extreme that they name: `routing`: each row names 2 different experts. Among the rows of one device (aligned blocks of 256 rows) no expert is named more than 160 times, and in every draw some expert is named exactly 160 times in some block.
All inputs are finite; a program needn't handle non-finite values.
Results may differ from a plain program's by a relative error of at most 0.02.
Values may be sent and summed in bfloat16 or wider, within the bound.
A program may use at most 128 MiB of HBM per device.

v0:
```python
import jax
import jax.numpy as jnp
from jax import lax
from jax.sharding import PartitionSpec as P


def per_device(tokens, cotangent, routing, group_gate, inner_gate, w_gate, w_up, w_down):
    expert_count = lax.axis_size("ep")
    tok_rows, model_width = tokens.shape
    top_k = routing.shape[1]
    capacity = tok_rows * top_k * 5 // (4 * expert_count)
    flat_route = routing.reshape(-1)
    one_hot = (flat_route[:, None] == jnp.arange(expert_count, dtype=jnp.int32)[None, :]).astype(
        jnp.int32
    )
    within = jnp.sum(one_hot * (jnp.cumsum(one_hot, axis=0) - 1), axis=1)
    slot_of = flat_route * capacity + within
    token_of = jnp.arange(tok_rows * top_k, dtype=jnp.int32) // top_k
    combine = (group_gate[:, None] * inner_gate).reshape(-1)
    send_weight = jnp.zeros((expert_count * capacity,), jnp.float32).at[slot_of].set(combine)

    def place_rows(source):
        empty = jnp.zeros((expert_count * capacity, source.shape[1]), source.dtype)
        return empty.at[slot_of].set(source[token_of])

    col_width = model_width // lax.axis_size("tp")
    offset = lax.axis_index("tp") * col_width
    token_cols = place_rows(lax.dynamic_slice_in_dim(tokens, offset, col_width, 1))
    cot_cols = place_rows(lax.dynamic_slice_in_dim(cotangent, offset, col_width, 1))
    token_cols, cot_cols, row_weight = (
        lax.all_to_all(token_cols, "ep", split_axis=0, concat_axis=0, tiled=True),
        lax.all_to_all(cot_cols, "ep", split_axis=0, concat_axis=0, tiled=True),
        lax.all_to_all(
            send_weight.astype(jnp.bfloat16), "ep", split_axis=0, concat_axis=0, tiled=True
        ).astype(send_weight.dtype),
    )
    rows_in, cot_rows = (
        lax.all_gather(token_cols, "tp", axis=1, tiled=True),
        lax.all_gather(cot_cols, "tp", axis=1, tiled=True),
    )
    gate_weight = w_gate[0]
    up_weight = w_up[0]
    down_weight = w_down[0]
    gate_pre = jnp.dot(rows_in, gate_weight, preferred_element_type=jnp.float32)
    up_pre = jnp.dot(rows_in, up_weight, preferred_element_type=jnp.float32)
    sigmoid_gate = jax.nn.sigmoid(gate_pre)
    silu_gate = gate_pre * sigmoid_gate
    hidden = (silu_gate * up_pre).astype(jnp.bfloat16)
    scaled_cot = (row_weight[:, None] * cot_rows).astype(jnp.bfloat16)
    down_grad = lax.dot_general(
        hidden, scaled_cot, (((0,), (0,)), ((), ())), preferred_element_type=jnp.float32
    )
    grad_hidden = lax.dot_general(
        cot_rows, down_weight, (((1,), (1,)), ((), ())), preferred_element_type=jnp.float32
    )
    partial_scores = jnp.sum(grad_hidden * hidden.astype(jnp.float32), axis=1)
    weighted = row_weight[:, None] * grad_hidden
    grad_gate_in = (
        weighted * up_pre * sigmoid_gate * (1.0 + gate_pre * (1.0 - sigmoid_gate))
    ).astype(jnp.bfloat16)
    grad_up_in = (weighted * silu_gate).astype(jnp.bfloat16)
    gate_grad = lax.dot_general(
        rows_in, grad_gate_in, (((0,), (0,)), ((), ())), preferred_element_type=jnp.float32
    )
    upper_grad = lax.dot_general(
        rows_in, grad_up_in, (((0,), (0,)), ((), ())), preferred_element_type=jnp.float32
    )
    partial_rows = lax.dot_general(
        grad_gate_in, gate_weight, (((1,), (1,)), ((), ())), preferred_element_type=jnp.float32
    ) + lax.dot_general(
        grad_up_in, up_weight, (((1,), (1,)), ((), ())), preferred_element_type=jnp.float32
    )
    row_grad = lax.psum_scatter(
        partial_rows.astype(jnp.bfloat16), "tp", scatter_dimension=1, tiled=True
    )
    scores = lax.psum(partial_scores, "tp")
    back_rows, back_scores = (
        lax.all_to_all(row_grad, "ep", split_axis=0, concat_axis=0, tiled=True),
        lax.all_to_all(
            scores.astype(jnp.bfloat16), "ep", split_axis=0, concat_axis=0, tiled=True
        ).astype(scores.dtype),
    )
    picked = back_rows[slot_of].astype(jnp.float32)
    token_grad = jnp.sum(picked.reshape(tok_rows, top_k, picked.shape[1]), axis=1).astype(
        jnp.bfloat16
    )
    score_of = back_scores[slot_of].reshape(tok_rows, top_k)
    inner_grad = group_gate[:, None] * score_of
    group_grad = jnp.sum(inner_gate * score_of, axis=1)
    return (
        token_grad,
        group_grad,
        inner_grad,
        gate_grad.astype(jnp.bfloat16)[None],
        upper_grad.astype(jnp.bfloat16)[None],
        down_grad.astype(jnp.bfloat16)[None],
    )


def solution(mesh):
    return jax.shard_map(
        per_device,
        mesh=mesh,
        in_specs=(
            P("ep", None),
            P("ep", None),
            P("ep", None),
            P("ep"),
            P("ep", None),
            P("ep", None, "tp"),
            P("ep", None, "tp"),
            P("ep", "tp", None),
        ),
        out_specs=(
            P("ep", "tp"),
            P("ep"),
            P("ep", None),
            P("ep", None, "tp"),
            P("ep", None, "tp"),
            P("ep", "tp", None),
        ),
        check_vma=False,
    )
```

profile of v0, /device:TPU:0, one launch (start us, length us, event | category | flops | bytes accessed | tf_op | source)
XLA Modules:
  0.0 238.5 jit_solution(333309969247349896)
XLA Ops:
  7.3 0.8 broadcast_multiply_fusion.2
  8.1 0.8 copy.21
  9.5 1.2 reduce-window.6
  10.7 0.2 slice_reduce_fusion
  11.3 1.1 constant_dynamic-slice_fusion
  12.3 4.9 %scatter_custom_fusion.2 = bf16[640,512]{1,0:T(8,128)(2,1)S(1)} fusion(s32[512]{0:T(512)S(1)} %bitcast.64, bf16[256,512]{1,0:T(8,128)(2,1)S(1)} %get-tuple-element.24, s32[1024]{0:T(1024)S(1)} %pad_clamp_fusion.1, bf16[]{:T(256)} %constant.39.clone.1), kind=kCustom, calls=%fused_computation.32 | custom fusion | bytes 655362 | tf_op jit(solution)/shard_map/scatter | solution.py:24
  17.2 15.0 %all_to_all.56 = bf16[4,160,512]{2,1,0:T(8,128)(2,1)} all-to-all(bf16[4,160,512]{2,1,0:T(8,128)(2,1)S(1)} %bitcast.62), channel_id=1, replica_groups=mesh['ep'=4,'tp'=8] {'ep'}, dimensions={0} | all-to-all | bytes 1310720 | tf_op jit(solution)/shard_map/all_to_all | solution.py:31
  32.3 4.9 %scatter_custom_fusion.1 = bf16[640,512]{1,0:T(8,128)(2,1)S(1)} fusion(s32[512]{0:T(512)S(1)} %bitcast.65, bf16[256,512]{1,0:T(8,128)(2,1)S(1)} %get-tuple-element.25, s32[1024]{0:T(1024)S(1)} %pad_clamp_fusion.1, bf16[]{:T(256)} %constant.39.clone.1), kind=kCustom, calls=%fused_computation.34 | custom fusion | bytes 655362 | tf_op jit(solution)/shard_map/scatter | solution.py:24
  37.2 11.8 %all_to_all.57 = bf16[4,160,512]{2,1,0:T(8,128)(2,1)} all-to-all(bf16[4,160,512]{2,1,0:T(8,128)(2,1)S(1)} %bitcast.61), channel_id=1, replica_groups=mesh['ep'=4,'tp'=8] {'ep'}, dimensions={0} | all-to-all | bytes 1310720 | tf_op jit(solution)/shard_map/all_to_all | solution.py:32
  49.5 2.4 %scatter_custom_fusion = f32[640]{0:T(1024)S(1)} fusion(s32[512]{0:T(512)S(1)} %bitcast.66, f32[512]{0:T(512)S(1)} %reshape.172, f32[]{:T(128)} %constant.17.clone.1), kind=kCustom, calls=%fused_computation.59 | custom fusion | bytes 2564 | tf_op jit(solution)/shard_map/scatter | solution.py:20
  52.1 7.0 %all_to_all.58 = bf16[4,160,1]{1,2,0:T(2,128)(2,1)S(1)} all-to-all(bf16[4,160,1]{1,2,0:T(2,128)(2,1)S(1)} %all_to_all.49), channel_id=1, replica_groups=mesh['ep'=4,'tp'=8] {'ep'}, dimensions={0} | all-to-all | bytes 2560 | tf_op jit(solution)/shard_map/all_to_all | solution.py:33
  59.2 28.9 %all-gather.5.cloned.1.call-done = bf16[640,4096]{1,0:T(8,128)(2,1)} async-done(((bf16[640,512]{1,0:T(8,128)(2,1)}), bf16[640,4096]{1,0:T(8,128)(2,1)}) %all-gather.5.cloned.1.call-update) | async-done | bytes 5242896 | tf_op jit(solution)/shard_map/all_gather | solution.py:38
  88.1 5.3 %fusion.8 = f32[640,256]{0,1:T(8,128)} fusion(bf16[640,4096]{1,0:T(8,128)(2,1)} %all-gather.5.cloned.1.call-done, bf16[1,4096,256]{2,1,0:T(8,128)(2,1)S(1)} %copy-done), kind=kOutput, calls=%fused_computation.19 | convolution fusion | flops 1342177280 | bytes 7995392 | tf_op jit(solution)/shard_map/dot_general | solution.py:44
  93.4 2.8 %fusion.11 = f32[640,256]{0,1:T(8,128)} fusion(bf16[640,4096]{1,0:T(8,128)(2,1)S(1)} %copy-done.5, bf16[1,4096,256]{2,1,0:T(8,128)(2,1)S(1)} %copy-done.1), kind=kOutput, calls=%fused_computation.22 | convolution fusion | flops 1342177280 | bytes 7995392 | tf_op jit(solution)/shard_map/dot_general | solution.py:45
  96.3 48.2 %all-gather.3.cloned.1.call-done = bf16[640,4096]{1,0:T(8,128)(2,1)} async-done(((bf16[640,512]{1,0:T(8,128)(2,1)}), bf16[640,4096]{1,0:T(8,128)(2,1)}) %all-gather.3.cloned.1.call-update) | async-done | bytes 5242896 | tf_op jit(solution)/shard_map/all_gather | solution.py:39
  144.5 5.4 %multiply_reduce_fusion = (f32[640]{0:T(1024)S(1)}, bf16[640,256]{0,1:T(8,128)(2,1)S(1)}, bf16[640,256]{0,1:T(8,128)(2,1)S(1)}, bf16[640,256]{0,1:T(8,128)(2,1)S(1)}) fusion(f32[640,256]{0,1:T(8,128)} %fusion.11, f32[640,256]{0,1:T(8,128)} %fusion.8, f32[640]{0:T(1024)S(1)} %reshape.134, bf16[640,4096]{1,0:T(8,128)(2,1)} %all-gather.3.cloned.1.call-done, ...), kind=kOutput, calls=%fused_computation.26 | convolution fusion | flops 1345289600 | bytes 9638912 | tf_op jit(solution)/shard_map/dot_general | solution.py:53
  149.9 1.6 fusion.6
  151.5 4.1 %add_convert_fusion = bf16[640,4096]{1,0:T(8,128)(2,1)} fusion(f32[640,4096]{1,0:T(8,128)S(1)} %fusion.6, bf16[640,256]{0,1:T(8,128)(2,1)S(1)} %get-tuple-element.21, bf16[1,4096,256]{2,1,0:T(8,128)(2,1)S(1)} %copy-done.2), kind=kOutput, calls=%fused_computation.8 | convolution fusion | flops 1347420160 | bytes 18153472 | tf_op jit(solution)/shard_map/dot_general | solution.py:70
  155.7 14.8 %psum.7 = bf16[640]{0:T(1024)(128)(2,1)S(1)} all-reduce(f32[640]{0:T(1024)S(1)} %get-tuple-element.18), channel_id=1, replica_groups=mesh['ep'=4,'tp'=8] {'tp'}, use_global_device_ids=true, to_apply=%region_9.10 | all-reduce | flops 640 | bytes 3840 | tf_op jit(solution)/shard_map/psum | solution.py:76
  170.5 0.7 all_to_all.50
  171.2 3.9 %all-to-all-start.4 = ((bf16[4,160,1]{1,2,0:T(2,128)(2,1)}), bf16[4,160,1]{1,2,0:T(2,128)(2,1)S(1)}, u32[]{:S(2)}, u32[]{:S(2)}) async-start(bf16[4,160,1]{1,2,0:T(2,128)(2,1)} %all_to_all.50), calls=%async_computation.5 | async-start | bytes 8192 | tf_op jit(solution)/shard_map/all_to_all | solution.py:79
  175.0 5.7 %fusion.5 = bf16[1,256,4096]{2,1,0:T(8,128)(2,1)} fusion(bf16[640,256]{0,1:T(8,128)(2,1)S(1)} %get-tuple-element.19, bf16[640,4096]{1,0:T(8,128)(2,1)} %all-gather.3.cloned.1.call-done, f32[640]{0:T(1024)S(1)} %reshape.134), kind=kOutput, calls=%fused_computation.16 | convolution fusion | flops 1351090176 | bytes 7670272 | tf_op jit(solution)/shard_map/dot_general | solution.py:50
  180.8 5.7 %fusion.3 = bf16[1,4096,256]{2,1,0:T(8,128)(2,1)} fusion(bf16[640,4096]{1,0:T(8,128)(2,1)} %all-gather.5.cloned.1.call-done, bf16[640,256]{0,1:T(8,128)(2,1)S(1)} %get-tuple-element.20), kind=kOutput, calls=%fused_computation.14 | convolution fusion | flops 1343225856 | bytes 7667712 | tf_op jit(solution)/shard_map/dot_general | solution.py:62
  186.5 28.0 %reduce-scatter.2.cloned.1.call-done = bf16[640,512]{1,0:T(8,128)(2,1)} async-done(((bf16[640,4096]{1,0:T(8,128)(2,1)}), bf16[640,512]{1,0:T(8,128)(2,1)}) %reduce-scatter.2.cloned.1.call-update) | async-done | bytes 655376 | tf_op jit(solution)/shard_map/reduce_scatter | solution.py:73
  214.5 3.6 %all-to-all-start.3 = ((bf16[4,160,512]{2,1,0:T(8,128)(2,1)}), bf16[4,160,512]{2,1,0:T(8,128)(2,1)S(1)}, u32[]{:S(2)}, u32[]{:S(2)}) async-start(bf16[4,160,512]{2,1,0:T(8,128)(2,1)} %bitcast.63), calls=%async_computation.4 | async-start | bytes 1310720 | tf_op jit(solution)/shard_map/all_to_all | solution.py:78
  218.2 5.7 %fusion.4 = bf16[1,4096,256]{2,1,0:T(8,128)(2,1)} fusion(bf16[640,4096]{1,0:T(8,128)(2,1)} %all-gather.5.cloned.1.call-done, bf16[640,256]{0,1:T(8,128)(2,1)S(1)} %get-tuple-element.21), kind=kOutput, calls=%fused_computation.15 | convolution fusion | flops 1343225856 | bytes 7667712 | tf_op jit(solution)/shard_map/dot_general | solution.py:65
  223.9 2.3 gather_fusion.1
  226.4 0.7 broadcast_multiply_fusion
  227.0 0.7 copy.27
  227.7 2.0 gather_fusion
  229.7 0.2 gather.17
  229.9 2.1 reduce_sum.43
  (42 shorter events, 1.9 us)
Async XLA Ops:
  7.2 81.0 %copy-start = (bf16[1,4096,256]{2,1,0:T(8,128)(2,1)S(1)}, bf16[1,4096,256]{2,1,0:T(8,128)(2,1)}, u32[]{:S(2)}) copy-start(bf16[1,4096,256]{2,1,0:T(8,128)(2,1)} %param.13) | copy-start | bytes 6291460
  7.2 41.9 %copy-start.4 = (f32[256,2]{0,1:T(2,128)S(1)}, f32[256,2]{0,1:T(2,128)}, u32[]{:S(2)}) copy-start(f32[256,2]{0,1:T(2,128)} %param.12) | copy-start | bytes 6148
  7.2 42.1 %copy-start.3 = (f32[256]{0:T(256)S(1)}, f32[256]{0:T(256)}, u32[]{:S(2)}) copy-start(f32[256]{0:T(256)} %param.11) | copy-start | bytes 3076
  7.2 80.9 %all-gather.5.cloned.1.call-start = ((), (), s32[]{:S(2)}) async-start(), calls=%async_computation.7 | async-start | bytes 5898240 | tf_op jit(solution)/shard_map/all_gather | solution.py:38
  32.3 112.2 %all-gather.3.cloned.1.call-start = ((), (), s32[]{:S(2)}) async-start(), calls=%async_computation.6 | async-start | bytes 5898240 | tf_op jit(solution)/shard_map/all_gather | solution.py:39
  49.1 165.4 %reduce-scatter.2.cloned.1.call-start = ((), (), s32[]{:S(2)}) async-start(), calls=%async_computation.8 | async-start | bytes 5898240 | tf_op jit(solution)/shard_map/reduce_scatter | solution.py:73
  88.1 5.3 %copy-start.1 = (bf16[1,4096,256]{2,1,0:T(8,128)(2,1)S(1)}, bf16[1,4096,256]{2,1,0:T(8,128)(2,1)}, u32[]{:S(2)}) copy-start(bf16[1,4096,256]{2,1,0:T(8,128)(2,1)} %param.14) | copy-start | bytes 6291460
  88.1 5.3 %copy-start.5 = (bf16[640,4096]{1,0:T(8,128)(2,1)S(1)}, bf16[640,4096]{1,0:T(8,128)(2,1)}, u32[]{:S(2)}) copy-start(bf16[640,4096]{1,0:T(8,128)(2,1)} %all-gather.5.cloned.1.call-done) | copy-start | bytes 15728644
  149.9 1.6 copy-start.2
  171.2 15.3 %all-to-all-start.4 = ((bf16[4,160,1]{1,2,0:T(2,128)(2,1)}), bf16[4,160,1]{1,2,0:T(2,128)(2,1)S(1)}, u32[]{:S(2)}, u32[]{:S(2)}) async-start(bf16[4,160,1]{1,2,0:T(2,128)(2,1)} %all_to_all.50), calls=%async_computation.5 | async-start | bytes 8192 | tf_op jit(solution)/shard_map/all_to_all | solution.py:79
  214.5 13.2 %all-to-all-start.3 = ((bf16[4,160,512]{2,1,0:T(8,128)(2,1)}), bf16[4,160,512]{2,1,0:T(8,128)(2,1)S(1)}, u32[]{:S(2)}, u32[]{:S(2)}) async-start(bf16[4,160,512]{2,1,0:T(8,128)(2,1)} %bitcast.63), calls=%async_computation.4 | async-start | bytes 1310720 | tf_op jit(solution)/shard_map/all_to_all | solution.py:78
Sparse Core Ops, SparseCore 0:
  32.4 55.6 all-gather.4
  89.7 54.7 all-gather.2
  155.8 58.7 reduce-scatter.1
where the time goes:
time: 239 us; the launch traced here: 238 us
  waiting for transfers between devices  105 us (44%)
  blocking collectives  48.7 us (20%)
  matrix products  36.3 us (15%)
  local copies, waits for them, and re-layouts  21.4 us (9%)
  between operations  14 us (6%)
  starting transfers between devices  7.63 us (3%)
  other arithmetic  5.27 us (2%)
    all_gather x1, waiting for transfers between devices, per_device(): lax.all_gather(cot_cols, 'tp', axis=1, tiled=True)  48.2 us
    all_gather x1, waiting for transfers between devices, per_device(): lax.all_gather(token_cols, 'tp', axis=1, tiled=True)  28.9 us
    reduce_scatter x1, waiting for transfers between devices, per_device(): lax.psum_scatter(partial_rows.astype(jnp.bfloat16), 'tp', scatter_dimensi...  28 us
    all_to_all x1, blocking collectives, per_device(): lax.all_to_all(token_cols, 'ep', split_axis=0, concat_axis=0, tiled=True)  15 us
    psum x1, blocking collectives, per_device(): scores = lax.psum(partial_scores, 'tp')  14.8 us
    all_to_all x1, blocking collectives, per_device(): lax.all_to_all(cot_cols, 'ep', split_axis=0, concat_axis=0, tiled=True)  11.8 us
    scatter x2, local copies, waits for them, and re-layouts, place_rows(): return empty.at[slot_of].set(source[token_of])  9.78 us
    all_to_all x1, blocking collectives, per_device(): lax.all_to_all(send_weight.astype(jnp.bfloat16), 'ep', split_axis=0, conc...  7.01 us
  transfers between devices with their start and end apart: 5, of which 3 were waited for; matrix products, arithmetic and copies ran while one was open for 15% of the time, Pallas kernels for 0%

commit v1 on v0

--- a/solution.py
+++ b/solution.py
@@ -2,6 +2,12 @@
 import jax.numpy as jnp
 from jax import lax
 from jax.sharding import PartitionSpec as P
+
+
+def summed_here(block, axis):
+    parts = lax.all_gather(block, axis, axis=0, tiled=False)
+    result = parts.sum(axis=0)
+    return result
 
 
 def per_device(tokens, cotangent, routing, group_gate, inner_gate, w_gate, w_up, w_down):
@@ -73,7 +79,7 @@
     row_grad = lax.psum_scatter(
         partial_rows.astype(jnp.bfloat16), "tp", scatter_dimension=1, tiled=True
     )
-    scores = lax.psum(partial_scores, "tp")
+    scores = summed_here(partial_scores, "tp")
     back_rows, back_scores = (
         lax.all_to_all(row_grad, "ep", split_axis=0, concat_axis=0, tiled=True),
         lax.all_to_all(

time: 239 us -> 240 us (level)
    psum x1 -> x0, blocking collectives: 14.8 us -> none  [per_device(): scores = lax.psum(partial_scores, 'tp')]
    all_gather x0 -> x1, blocking collectives: none -> 14.2 us  [summed_here(): parts = lax.all_gather(block, axis, axis=0, tiled=False)]
  transfers between devices with their start and end apart: 5 -> 5, of which waited for: 3 -> 3; matrix products, arithmetic and copies ran while one was open for 15% -> 16% of each run, Pallas kernels for 0% -> 0%
where the time goes in v1:
time: 240 us; the launch traced here: 239 us
  waiting for transfers between devices  106 us (44%)
  blocking collectives  48.1 us (20%)
  matrix products  37.2 us (16%)
  local copies, waits for them, and re-layouts  21.4 us (9%)
  between operations  14 us (6%)
  starting transfers between devices  7.42 us (3%)
  other arithmetic  5.3 us (2%)
    all_gather x1, waiting for transfers between devices, per_device(): lax.all_gather(cot_cols, 'tp', axis=1, tiled=True)  48.2 us
    all_gather x1, waiting for transfers between devices, per_device(): lax.all_gather(token_cols, 'tp', axis=1, tiled=True)  28.9 us
    reduce_scatter x1, waiting for transfers between devices, per_device(): lax.psum_scatter(partial_rows.astype(jnp.bfloat16), 'tp', scatter_dimensi...  28.6 us
    all_to_all x1, blocking collectives, per_device(): lax.all_to_all(token_cols, 'ep', split_axis=0, concat_axis=0, tiled=True)  15 us
    all_gather x1, blocking collectives, summed_here(): parts = lax.all_gather(block, axis, axis=0, tiled=False)  14.2 us
    all_to_all x1, blocking collectives, per_device(): lax.all_to_all(cot_cols, 'ep', split_axis=0, concat_axis=0, tiled=True)  11.8 us
    scatter x2, local copies, waits for them, and re-layouts, place_rows(): return empty.at[slot_of].set(source[token_of])  9.78 us
    all_to_all x1, blocking collectives, per_device(): lax.all_to_all(send_weight.astype(jnp.bfloat16), 'ep', split_axis=0, conc...  7.01 us
  transfers between devices with their start and end apart: 5, of which 3 were waited for; matrix products, arithmetic and copies ran while one was open for 16% of the time, Pallas kernels for 0%

profile of v1, /device:TPU:0, one launch (start us, length us, event | category | flops | bytes accessed | tf_op | source)
XLA Modules:
  0.0 239.1 jit_solution(16147345241928082204)
XLA Ops:
  7.3 0.8 broadcast_multiply_fusion.2
  8.1 0.8 copy.21
  9.5 1.2 reduce-window.6
  10.7 0.2 slice_reduce_fusion
  11.3 1.1 constant_dynamic-slice_fusion
  12.3 4.9 %scatter_custom_fusion.2 = bf16[640,512]{1,0:T(8,128)(2,1)S(1)} fusion(s32[512]{0:T(512)S(1)} %bitcast.64, bf16[256,512]{1,0:T(8,128)(2,1)S(1)} %get-tuple-element.24, s32[1024]{0:T(1024)S(1)} %pad_clamp_fusion.1, bf16[]{:T(256)} %constant.39.clone.1), kind=kCustom, calls=%fused_computation.32 | custom fusion | bytes 655362 | tf_op jit(solution)/shard_map/scatter | solution.py:30
  17.2 15.0 %all_to_all.52 = bf16[4,160,512]{2,1,0:T(8,128)(2,1)} all-to-all(bf16[4,160,512]{2,1,0:T(8,128)(2,1)S(1)} %bitcast.62), channel_id=1, replica_groups=mesh['ep'=4,'tp'=8] {'ep'}, dimensions={0} | all-to-all | bytes 1310720 | tf_op jit(solution)/shard_map/all_to_all | solution.py:37
  32.3 4.9 %scatter_custom_fusion.1 = bf16[640,512]{1,0:T(8,128)(2,1)S(1)} fusion(s32[512]{0:T(512)S(1)} %bitcast.65, bf16[256,512]{1,0:T(8,128)(2,1)S(1)} %get-tuple-element.25, s32[1024]{0:T(1024)S(1)} %pad_clamp_fusion.1, bf16[]{:T(256)} %constant.39.clone.1), kind=kCustom, calls=%fused_computation.34 | custom fusion | bytes 655362 | tf_op jit(solution)/shard_map/scatter | solution.py:30
  37.2 11.8 %all_to_all.53 = bf16[4,160,512]{2,1,0:T(8,128)(2,1)} all-to-all(bf16[4,160,512]{2,1,0:T(8,128)(2,1)S(1)} %bitcast.61), channel_id=1, replica_groups=mesh['ep'=4,'tp'=8] {'ep'}, dimensions={0} | all-to-all | bytes 1310720 | tf_op jit(solution)/shard_map/all_to_all | solution.py:38
  49.5 2.4 %scatter_custom_fusion = f32[640]{0:T(1024)S(1)} fusion(s32[512]{0:T(512)S(1)} %bitcast.66, f32[512]{0:T(512)S(1)} %reshape.183, f32[]{:T(128)} %constant.17.clone.1), kind=kCustom, calls=%fused_computation.59 | custom fusion | bytes 2564 | tf_op jit(solution)/shard_map/scatter | solution.py:26
  52.1 7.0 %all_to_all.54 = bf16[4,160,1]{1,2,0:T(2,128)(2,1)S(1)} all-to-all(bf16[4,160,1]{1,2,0:T(2,128)(2,1)S(1)} %all_to_all.46), channel_id=1, replica_groups=mesh['ep'=4,'tp'=8] {'ep'}, dimensions={0} | all-to-all | bytes 2560 | tf_op jit(solution)/shard_map/all_to_all | solution.py:39
  59.2 28.9 %all-gather.7.cloned.1.call-done = bf16[640,4096]{1,0:T(8,128)(2,1)} async-done(((bf16[640,512]{1,0:T(8,128)(2,1)}), bf16[640,4096]{1,0:T(8,128)(2,1)}) %all-gather.7.cloned.1.call-update) | async-done | bytes 5242896 | tf_op jit(solution)/shard_map/all_gather | solution.py:44
  88.1 5.3 %fusion.8 = f32[640,256]{0,1:T(8,128)} fusion(bf16[640,4096]{1,0:T(8,128)(2,1)} %all-gather.7.cloned.1.call-done, bf16[1,4096,256]{2,1,0:T(8,128)(2,1)S(1)} %copy-done), kind=kOutput, calls=%fused_computation.19 | convolution fusion | flops 1342177280 | bytes 7995392 | tf_op jit(solution)/shard_map/dot_general | solution.py:50
  93.4 2.8 %fusion.11 = f32[640,256]{0,1:T(8,128)} fusion(bf16[640,4096]{1,0:T(8,128)(2,1)S(1)} %copy-done.5, bf16[1,4096,256]{2,1,0:T(8,128)(2,1)S(1)} %copy-done.1), kind=kOutput, calls=%fused_computation.22 | convolution fusion | flops 1342177280 | bytes 7995392 | tf_op jit(solution)/shard_map/dot_general | solution.py:51
  96.3 48.2 %all-gather.5.cloned.1.call-done = bf16[640,4096]{1,0:T(8,128)(2,1)} async-done(((bf16[640,512]{1,0:T(8,128)(2,1)}), bf16[640,4096]{1,0:T(8,128)(2,1)}) %all-gather.5.cloned.1.call-update) | async-done | bytes 5242896 | tf_op jit(solution)/shard_map/all_gather | solution.py:45
  144.5 6.1 %multiply_reduce_fusion = (f32[640]{0:T(1024)S(1)}, bf16[640,256]{0,1:T(8,128)(2,1)}, bf16[640,256]{0,1:T(8,128)(2,1)S(1)}, bf16[640,256]{0,1:T(8,128)(2,1)S(1)}) fusion(f32[640,256]{0,1:T(8,128)} %fusion.11, f32[640,256]{0,1:T(8,128)} %fusion.8, f32[640]{0:T(1024)S(1)} %reshape.145, bf16[640,4096]{1,0:T(8,128)(2,1)} %all-gather.5.cloned.1.call-done, ...), kind=kOutput, calls=%fused_computation.26 | convolution fusion | flops 1345289600 | bytes 9638912 | tf_op jit(solution)/shard_map/dot_general | solution.py:59
  150.6 1.6 fusion.6
  152.2 4.1 %add_convert_fusion = bf16[640,4096]{1,0:T(8,128)(2,1)} fusion(f32[640,4096]{1,0:T(8,128)S(1)} %fusion.6, bf16[640,256]{0,1:T(8,128)(2,1)S(1)} %get-tuple-element.21, bf16[1,4096,256]{2,1,0:T(8,128)(2,1)S(1)} %copy-done.2), kind=kOutput, calls=%fused_computation.8 | convolution fusion | flops 1347420160 | bytes 18153472 | tf_op jit(solution)/shard_map/dot_general | solution.py:76
  156.4 14.2 %all-gather.1 = f32[8,1,640]{2,1,0:T(1,128)S(1)} all-gather(f32[1,1,640]{2,1,0:T(1,128)S(1)} %reshape.204), channel_id=2, replica_groups=mesh['ep'=4,'tp'=8] {'tp'}, dimensions={0}, use_global_device_ids=true | all-gather | bytes 23040 | tf_op jit(solution)/shard_map/all_gather | solution.py:8
  170.6 0.7 convert_element_type.90
  171.3 3.6 %all-to-all-start.4 = ((bf16[4,160,1]{1,2,0:T(2,128)(2,1)}), bf16[4,160,1]{1,2,0:T(2,128)(2,1)S(1)}, u32[]{:S(2)}, u32[]{:S(2)}) async-start(bf16[4,160,1]{1,2,0:T(2,128)(2,1)} %convert_element_type.90), calls=%async_computation.5 | async-start | bytes 8192 | tf_op jit(solution)/shard_map/all_to_all | solution.py:85
  174.9 5.9 %fusion.5 = bf16[1,256,4096]{2,1,0:T(8,128)(2,1)} fusion(bf16[640,256]{0,1:T(8,128)(2,1)} %get-tuple-element.19, bf16[640,4096]{1,0:T(8,128)(2,1)} %all-gather.5.cloned.1.call-done, f32[640]{0:T(1024)S(1)} %reshape.145), kind=kOutput, calls=%fused_computation.16 | convolution fusion | flops 1351090176 | bytes 7670272 | tf_op jit(solution)/shard_map/dot_general | solution.py:56
  180.8 5.7 %fusion.3 = bf16[1,4096,256]{2,1,0:T(8,128)(2,1)} fusion(bf16[640,4096]{1,0:T(8,128)(2,1)} %all-gather.7.cloned.1.call-done, bf16[640,256]{0,1:T(8,128)(2,1)S(1)} %get-tuple-element.20), kind=kOutput, calls=%fused_computation.14 | convolution fusion | flops 1343225856 | bytes 7667712 | tf_op jit(solution)/shard_map/dot_general | solution.py:68
  186.5 28.6 %reduce-scatter.2.cloned.1.call-done = bf16[640,512]{1,0:T(8,128)(2,1)} async-done(((bf16[640,4096]{1,0:T(8,128)(2,1)}), bf16[640,512]{1,0:T(8,128)(2,1)}) %reduce-scatter.2.cloned.1.call-update) | async-done | bytes 655376 | tf_op jit(solution)/shard_map/reduce_scatter | solution.py:79
  215.1 3.7 %all-to-all-start.3 = ((bf16[4,160,512]{2,1,0:T(8,128)(2,1)}), bf16[4,160,512]{2,1,0:T(8,128)(2,1)S(1)}, u32[]{:S(2)}, u32[]{:S(2)}) async-start(bf16[4,160,512]{2,1,0:T(8,128)(2,1)} %bitcast.63), calls=%async_computation.4 | async-start | bytes 1310720 | tf_op jit(solution)/shard_map/all_to_all | solution.py:84
  218.8 5.7 %fusion.4 = bf16[1,4096,256]{2,1,0:T(8,128)(2,1)} fusion(bf16[640,4096]{1,0:T(8,128)(2,1)} %all-gather.7.cloned.1.call-done, bf16[640,256]{0,1:T(8,128)(2,1)S(1)} %get-tuple-element.21), kind=kOutput, calls=%fused_computation.15 | convolution fusion | flops 1343225856 | bytes 7667712 | tf_op jit(solution)/shard_map/dot_general | solution.py:71
  224.6 2.3 gather_fusion.1
  227.0 0.7 broadcast_multiply_fusion
  227.7 0.7 copy.27
  228.4 2.0 gather_fusion
  230.3 0.2 gather.17
  230.5 2.1 reduce_sum.52
  (44 shorter events, 1.9 us)
Async XLA Ops:
  7.2 81.0 %copy-start = (bf16[1,4096,256]{2,1,0:T(8,128)(2,1)S(1)}, bf16[1,4096,256]{2,1,0:T(8,128)(2,1)}, u32[]{:S(2)}) copy-start(bf16[1,4096,256]{2,1,0:T(8,128)(2,1)} %param.13) | copy-start | bytes 6291460
  7.2 41.9 %copy-start.4 = (f32[256,2]{0,1:T(2,128)S(1)}, f32[256,2]{0,1:T(2,128)}, u32[]{:S(2)}) copy-start(f32[256,2]{0,1:T(2,128)} %param.12) | copy-start | bytes 6148
  7.2 42.1 %copy-start.3 = (f32[256]{0:T(256)S(1)}, f32[256]{0:T(256)}, u32[]{:S(2)}) copy-start(f32[256]{0:T(256)} %param.11) | copy-start | bytes 3076
  7.2 80.9 %all-gather.7.cloned.1.call-start = ((), (), s32[]{:S(2)}) async-start(), calls=%async_computation.7 | async-start | bytes 5898240 | tf_op jit(solution)/shard_map/all_gather | solution.py:44
  32.3 112.2 %all-gather.5.cloned.1.call-start = ((), (), s32[]{:S(2)}) async-start(), calls=%async_computation.6 | async-start | bytes 5898240 | tf_op jit(solution)/shard_map/all_gather | solution.py:45
  49.1 166.1 %reduce-scatter.2.cloned.1.call-start = ((), (), s32[]{:S(2)}) async-start(), calls=%async_computation.8 | async-start | bytes 5898240 | tf_op jit(solution)/shard_map/reduce_scatter | solution.py:79
  88.1 5.3 %copy-start.1 = (bf16[1,4096,256]{2,1,0:T(8,128)(2,1)S(1)}, bf16[1,4096,256]{2,1,0:T(8,128)(2,1)}, u32[]{:S(2)}) copy-start(bf16[1,4096,256]{2,1,0:T(8,128)(2,1)} %param.14) | copy-start | bytes 6291460
  88.1 5.3 %copy-start.5 = (bf16[640,4096]{1,0:T(8,128)(2,1)S(1)}, bf16[640,4096]{1,0:T(8,128)(2,1)}, u32[]{:S(2)}) copy-start(bf16[640,4096]{1,0:T(8,128)(2,1)} %all-gather.7.cloned.1.call-done) | copy-start | bytes 15728644
  150.6 1.6 copy-start.2
  171.3 15.2 %all-to-all-start.4 = ((bf16[4,160,1]{1,2,0:T(2,128)(2,1)}), bf16[4,160,1]{1,2,0:T(2,128)(2,1)S(1)}, u32[]{:S(2)}, u32[]{:S(2)}) async-start(bf16[4,160,1]{1,2,0:T(2,128)(2,1)} %convert_element_type.90), calls=%async_computation.5 | async-start | bytes 8192 | tf_op jit(solution)/shard_map/all_to_all | solution.py:85
  215.1 13.2 %all-to-all-start.3 = ((bf16[4,160,512]{2,1,0:T(8,128)(2,1)}), bf16[4,160,512]{2,1,0:T(8,128)(2,1)S(1)}, u32[]{:S(2)}, u32[]{:S(2)}) async-start(bf16[4,160,512]{2,1,0:T(8,128)(2,1)} %bitcast.63), calls=%async_computation.4 | async-start | bytes 1310720 | tf_op jit(solution)/shard_map/all_to_all | solution.py:84
Sparse Core Ops, SparseCore 0:
  32.4 55.6 all-gather.6
  89.7 54.7 all-gather.4
  156.5 58.6 reduce-scatter.1
